TPU v7x, 32 devices: a whole 2x2x4 slice. The times are simulated.
32 devices in a mesh: sp: 4 (over z), dp: 8 (over y, x, core).
Axes of the slice: x: 2, y: 2, z: 4, core: 2. Of those that a mesh axis runs over, the one named last changes fastest.
Arguments:
- queries: bfloat16 [8, 768, 1024], P('dp', 'sp'), may hold values from -6 to 6
- keys: bfloat16 [8, 768, 256], P('dp', 'sp'), may hold values from -6 to 6
- values: bfloat16 [8, 768, 256], P('dp', 'sp'), may hold values from -6 to 6
- query_gain: float32 [64], replicated, may hold values from 0.15 to 7
- key_gain: float32 [64], replicated, may hold values from 0.15 to 7
- out_weight: bfloat16 [1024, 2048], P(None, 'dp'), may hold values from -0.1875 to 0.1875
- out_gain: float32 [2048], replicated, may hold values from 0.1 to 1.9
Outputs:
- output: bfloat16 [8, 768, 2048], P('dp', 'sp')
All inputs are finite; a program needn't handle non-finite values.
Results may differ from a plain program's by a relative error of at most 0.0035.
The roundings to bfloat16 on the way count: a program that leaves them out, or rounds other values in their place, can miss the bound.
Values may be sent and summed in bfloat16 or wider, within the bound.
A program may use at most 64 MiB of HBM per device.

v0:
```python
import jax
import jax.numpy as jnp
from jax import lax
from jax.sharding import PartitionSpec as P

QH = 16
KVH = 4
HEAD = 64
GRID_W = 64


EPSILON = 1e-06
ROTARY_BASE = 10000.0


def rotate(vectors, positions, width):
    half_width = width // 2
    frequency = ROTARY_BASE ** (-jnp.arange(0, width, 2, dtype=jnp.float32) / width)
    angles = positions.astype(jnp.float32)[:, None] * frequency[None, :]
    cosines = jnp.cos(angles)[:, None, :]
    sine_table = jnp.sin(angles)[:, None, :]
    first_half = vectors[..., :half_width]
    second_half = vectors[..., half_width:]
    return jnp.concatenate(
        [
            first_half * cosines - second_half * sine_table,
            second_half * cosines + first_half * sine_table,
        ],
        axis=-1,
    )


def prepare(vectors, gain_vector, grid_row, grid_col):
    vectors = vectors.astype(jnp.float32)
    vectors = (
        vectors
        * lax.rsqrt(jnp.mean(vectors * vectors, axis=-1, keepdims=True) + EPSILON)
        * gain_vector
    )
    half_width = HEAD // 2
    turned = jnp.concatenate(
        [
            rotate(vectors[..., :half_width], grid_row, half_width),
            rotate(vectors[..., half_width:], grid_col, half_width),
        ],
        axis=-1,
    )
    return turned.astype(jnp.bfloat16)


def softmax_rows(scores):
    row_max = jnp.max(scores, axis=-1, keepdims=True)
    exponent = jnp.exp(scores - row_max)
    return exponent / jnp.sum(exponent, axis=-1, keepdims=True)


def per_device(queries, keys, values, query_gain, key_gain, out_weight, out_gain):
    sp_count = lax.axis_size("sp")
    tokens_here = queries.shape[1]
    seq_len = tokens_here * sp_count
    score_scale = HEAD ** (-0.5)
    offset = lax.axis_index("sp") * tokens_here
    positions = offset + jnp.arange(tokens_here, dtype=jnp.int32)
    grid_row = positions // GRID_W
    grid_col = positions % GRID_W
    query_rot = prepare(queries[0].reshape(tokens_here, QH, HEAD), query_gain, grid_row, grid_col)
    key_rot = prepare(keys[0].reshape(tokens_here, KVH, HEAD), key_gain, grid_row, grid_col)
    value_heads = values[0].reshape(tokens_here, KVH, HEAD)
    kv_pairs = jnp.concatenate([key_rot, value_heads], axis=2)
    all_pairs = lax.all_gather(
        kv_pairs.reshape(tokens_here, KVH * 2 * HEAD), "sp", axis=0, tiled=True
    )
    all_pairs = all_pairs.reshape(seq_len, KVH, 2, HEAD)
    key_all = all_pairs[:, :, 0].transpose(1, 0, 2)
    value_all = all_pairs[:, :, 1].transpose(1, 0, 2)
    query_groups = query_rot.reshape(tokens_here, KVH, QH // KVH, HEAD).transpose(1, 0, 2, 3)

    def attend_group(operands):
        query_group, key_head, value_head = operands
        scores = (
            jnp.einsum("qgd,kd->gqk", query_group, key_head, preferred_element_type=jnp.float32)
            * score_scale
        )
        attn_weights = softmax_rows(scores).astype(jnp.bfloat16)
        return jnp.einsum(
            "gqk,kd->qgd", attn_weights, value_head, preferred_element_type=jnp.float32
        ).astype(jnp.bfloat16)

    results = lax.map(attend_group, (query_groups, key_all, value_all))
    attended = results.transpose(1, 0, 2, 3).reshape(tokens_here, QH * HEAD)
    projected = jnp.dot(
        attended,
        lax.all_gather(out_weight, "dp", axis=1, tiled=True),
        preferred_element_type=jnp.float32,
    )
    normed = (
        projected
        * lax.rsqrt(jnp.mean(projected * projected, axis=-1, keepdims=True) + EPSILON)
        * out_gain
    )
    return normed.astype(jnp.bfloat16)[None]


def solution(mesh):
    return jax.shard_map(
        per_device,
        mesh=mesh,
        in_specs=(
            P("dp", "sp", None),
            P("dp", "sp", None),
            P("dp", "sp", None),
            P(),
            P(),
            P(None, "dp"),
            P(),
        ),
        out_specs=P("dp", "sp", None),
        check_vma=False,
    )
```

profile of v0, /device:TPU:0, one launch (start us, length us, event | category | flops | bytes accessed | tf_op | source)
XLA Modules:
  0.0 63.6 jit_solution(6471793219712596155)
XLA Ops:
  6.5 0.7 %all-gather.2.cloned.1.call-update = ((bf16[1024,256]{1,0:T(8,128)(2,1)}), bf16[1024,2048]{1,0:T(8,128)(2,1)}) async-update(((), (), s32[]{:S(2)}) %all-gather.2.cloned.1.call-start, bf16[1024,256]{1,0:T(8,128)(2,1)} %param.14) | async-update | bytes 5242904
  7.3 1.2 %copy.20 = bf16[1,192,1024]{1,2,0:T(8,128)(2,1)S(1)} copy(bf16[1,192,1024]{2,1,0:T(8,128)(2,1)} %param.9) | data formatting | bytes 786432 | tf_op args[0]
  8.5 1.0 %copy.16 = bf16[1,192,256]{1,2,0:T(8,128)(2,1)S(1)} copy(bf16[1,192,256]{2,1,0:T(8,128)(2,1)} %param.10) | data formatting | bytes 196608 | tf_op args[1]
  9.5 1.0 %copy.17 = bf16[1,192,256]{1,2,0:T(8,128)(2,1)S(1)} copy(bf16[1,192,256]{2,1,0:T(8,128)(2,1)} %param.11) | data formatting | bytes 196608 | tf_op args[2]
  10.6 0.2 multiply_cosine_fusion
  10.8 0.7 %fusion.44 = f32[192,4,64]{0,2,1:T(8,128)S(1)} fusion(bf16[192,4,64]{0,2,1:T(8,128)(2,1)S(1)} %bitcast.88, f32[64]{0:T(128)} %param.13, f32[192,4]{0,1:T(4,128)S(1)} %add_rsqrt_fusion.1), kind=kLoop, calls=%fused_computation.41 | loop fusion | flops 147456 | bytes 298240 | tf_op jit(solution)/shard_map/mul | solution.py:36
  11.6 0.1 copy.18
  11.8 21.3 %all_gather.6 = bf16[768,512]{1,0:T(8,128)(2,1)S(1)} all-gather(bf16[192,512]{1,0:T(8,128)(2,1)S(1)} %copy.18), channel_id=1, replica_groups=mesh['sp'=4,'dp'=8] {'sp'}, dimensions={0}, use_global_device_ids=true | all-gather | bytes 983040 | tf_op jit(solution)/shard_map/all_gather | solution.py:70
  33.1 0.3 copy.19
  33.4 0.1 fusion.40
  33.5 0.2 fusion.41
  33.7 0.2 subtract_convert_fusion.1
  33.9 0.1 maximum_bitcast_fusion
  34.1 18.3 %while.10 = (s32[]{:T(128)}, bf16[4,192,4,64]{1,3,2,0:T(8,128)(2,1)S(1)}, bf16[4,768,64]{1,2,0:T(8,128)(2,1)S(1)}, bf16[4,768,64]{1,2,0:T(8,128)(2,1)S(1)}, bf16[4,192,4,64]{1,3,2,0:T(8,128)(2,1)S(1)}, /*index=5*/s32[]{:T(128)}) while((s32[]{:T(128)}, bf16[4,192,4,64]{1,3,2,0:T(8,128)(2,1)S(1)}, bf16[4,768,64]{1,2,0:T(8,128)(2,1)S(1)}, ...), condition=%wide.region_5.6_spmd, body=%wide.region_2.5_spmd.sunk | while | flops 153993984 | bytes 5186629 | solution.py:89
  34.1 2.3 %fusion.71 = (f32[4,192]{1,0:T(4,128)S(1)}, f32[4,192,768]{2,1,0:T(8,128)}) fusion(bf16[4,192,4,64]{1,3,2,0:T(8,128)(2,1)S(1)} %get-tuple-element.114, s32[]{:T(128)} %get-tuple-element.104, bf16[4,768,64]{1,2,0:T(8,128)(2,1)S(1)} %get-tuple-element.113), kind=kOutput, calls=%fused_computation.73.clone.1 | convolution fusion | flops 77267712 | bytes 2592768 | tf_op jit(solution)/shard_map/while/body/eval_jaxpr/sub | solution.py:53
  36.4 2.2 %fusion.72 = bf16[4,192,4,64]{1,3,2,0:T(8,128)(2,1)S(1)} fusion(bf16[4,192,4,64]{1,3,2,0:T(8,128)(2,1)S(1)} %get-tuple-element.105, s32[]{:T(128)} %get-tuple-element.104, f32[4,192,768]{2,1,0:T(8,128)} %get-tuple-element.96, f32[4,192]{1,0:T(4,128)S(1)} %get-tuple-element.97, bf16[4,768,64]{1,2,0:T(8,128)(2,1)S(1)} %get-tuple-element.112), kind=kOutput, calls=%fused_computation.11.clone.1 | convolution fusion | flops 76726272 | bytes 2593792 | tf_op jit(solution)/shard_map/while/body/eval_jaxpr/gqk,kd->qgd/dot_general | solution.py:85
  38.6 2.3 %fusion.71 = (f32[4,192]{1,0:T(4,128)S(1)}, f32[4,192,768]{2,1,0:T(8,128)}) fusion(bf16[4,192,4,64]{1,3,2,0:T(8,128)(2,1)S(1)} %get-tuple-element.114, s32[]{:T(128)} %get-tuple-element.104, bf16[4,768,64]{1,2,0:T(8,128)(2,1)S(1)} %get-tuple-element.113), kind=kOutput, calls=%fused_computation.73.clone.1 | convolution fusion | flops 77267712 | bytes 2592768 | tf_op jit(solution)/shard_map/while/body/eval_jaxpr/sub | solution.py:53
  40.9 2.2 %fusion.72 = bf16[4,192,4,64]{1,3,2,0:T(8,128)(2,1)S(1)} fusion(bf16[4,192,4,64]{1,3,2,0:T(8,128)(2,1)S(1)} %get-tuple-element.105, s32[]{:T(128)} %get-tuple-element.104, f32[4,192,768]{2,1,0:T(8,128)} %get-tuple-element.96, f32[4,192]{1,0:T(4,128)S(1)} %get-tuple-element.97, bf16[4,768,64]{1,2,0:T(8,128)(2,1)S(1)} %get-tuple-element.112), kind=kOutput, calls=%fused_computation.11.clone.1 | convolution fusion | flops 76726272 | bytes 2593792 | tf_op jit(solution)/shard_map/while/body/eval_jaxpr/gqk,kd->qgd/dot_general | solution.py:85
  43.2 2.3 %fusion.71 = (f32[4,192]{1,0:T(4,128)S(1)}, f32[4,192,768]{2,1,0:T(8,128)}) fusion(bf16[4,192,4,64]{1,3,2,0:T(8,128)(2,1)S(1)} %get-tuple-element.114, s32[]{:T(128)} %get-tuple-element.104, bf16[4,768,64]{1,2,0:T(8,128)(2,1)S(1)} %get-tuple-element.113), kind=kOutput, calls=%fused_computation.73.clone.1 | convolution fusion | flops 77267712 | bytes 2592768 | tf_op jit(solution)/shard_map/while/body/eval_jaxpr/sub | solution.py:53
  45.5 2.2 %fusion.72 = bf16[4,192,4,64]{1,3,2,0:T(8,128)(2,1)S(1)} fusion(bf16[4,192,4,64]{1,3,2,0:T(8,128)(2,1)S(1)} %get-tuple-element.105, s32[]{:T(128)} %get-tuple-element.104, f32[4,192,768]{2,1,0:T(8,128)} %get-tuple-element.96, f32[4,192]{1,0:T(4,128)S(1)} %get-tuple-element.97, bf16[4,768,64]{1,2,0:T(8,128)(2,1)S(1)} %get-tuple-element.112), kind=kOutput, calls=%fused_computation.11.clone.1 | convolution fusion | flops 76726272 | bytes 2593792 | tf_op jit(solution)/shard_map/while/body/eval_jaxpr/gqk,kd->qgd/dot_general | solution.py:85
  47.8 2.3 %fusion.71 = (f32[4,192]{1,0:T(4,128)S(1)}, f32[4,192,768]{2,1,0:T(8,128)}) fusion(bf16[4,192,4,64]{1,3,2,0:T(8,128)(2,1)S(1)} %get-tuple-element.114, s32[]{:T(128)} %get-tuple-element.104, bf16[4,768,64]{1,2,0:T(8,128)(2,1)S(1)} %get-tuple-element.113), kind=kOutput, calls=%fused_computation.73.clone.1 | convolution fusion | flops 77267712 | bytes 2592768 | tf_op jit(solution)/shard_map/while/body/eval_jaxpr/sub | solution.py:53
  50.1 2.2 %fusion.72 = bf16[4,192,4,64]{1,3,2,0:T(8,128)(2,1)S(1)} fusion(bf16[4,192,4,64]{1,3,2,0:T(8,128)(2,1)S(1)} %get-tuple-element.105, s32[]{:T(128)} %get-tuple-element.104, f32[4,192,768]{2,1,0:T(8,128)} %get-tuple-element.96, f32[4,192]{1,0:T(4,128)S(1)} %get-tuple-element.97, bf16[4,768,64]{1,2,0:T(8,128)(2,1)S(1)} %get-tuple-element.112), kind=kOutput, calls=%fused_computation.11.clone.1 | convolution fusion | flops 76726272 | bytes 2593792 | tf_op jit(solution)/shard_map/while/body/eval_jaxpr/gqk,kd->qgd/dot_general | solution.py:85
  52.4 3.3 %multiply_reduce_fusion = (f32[192]{0:T(256)S(1)}, f32[192,2048]{1,0:T(8,128)S(1)}) fusion(bf16[192,1024]{0,1:T(8,128)(2,1)S(1)} %bitcast.94, bf16[1024,2048]{1,0:T(8,128)(2,1)} %all-gather.2.cloned.1.call-done), kind=kOutput, calls=%fused_computation.29 | convolution fusion | flops 806092608 | bytes 6161152 | tf_op jit(solution)/shard_map/dot_general | solution.py:91
  55.7 1.1 %fusion.42 = bf16[1,192,2048]{2,1,0:T(8,128)(2,1)} fusion(f32[192,2048]{1,0:T(8,128)S(1)} %get-tuple-element.60, f32[2048]{0:T(1024)S(1)} %copy-done, f32[192]{0:T(256)S(1)} %add_rsqrt_fusion.2), kind=kLoop, calls=%fused_computation.34 | loop fusion | flops 1179648 | bytes 2368256 | tf_op jit(solution)/shard_map/broadcast_in_dim | solution.py:101
  (19 shorter events, 0.3 us)
Async XLA Ops:
  6.5 45.8 %all-gather.2.cloned.1.call-start = ((), (), s32[]{:S(2)}) async-start(), calls=%async_computation | async-start | bytes 4718592 | tf_op jit(solution)/shard_map/all_gather | solution.py:93
  11.5 22.0 %copy-start.1 = (f32[64]{0:T(128)S(1)}, f32[64]{0:T(128)}, u32[]{:S(2)}) copy-start(f32[64]{0:T(128)} %param.12) | copy-start | bytes 772
  52.4 3.3 %copy-start = (f32[2048]{0:T(1024)S(1)}, f32[2048]{0:T(1024)}, u32[]{:S(2)}) copy-start(f32[2048]{0:T(1024)} %param.15) | copy-start | bytes 24580
Sparse Core Ops, SparseCore 0:
  9.2 40.0 all-gather.1
where the time goes:
time: 64 us; the launch traced here: 63.6 us
  matrix products  21.5 us (34%)
  blocking collectives  21.3 us (33%)
  between operations  13.6 us (21%)
  local copies, waits for them, and re-layouts  3.66 us (6%)
  other arithmetic  2.76 us (4%)
  waiting for transfers between devices  0.73 us (1%)
    all_gather x1, blocking collectives, per_device(): lax.all_gather(kv_pairs.reshape(tokens_here, KVH * 2 * HEAD), 'sp', axis=...  21.3 us
    sub x4, matrix products, softmax_rows(): exponent = jnp.exp(scores - row_max)  9.24 us
    dot_general x4, matrix products, attend_group(): jnp.einsum('gqk,kd->qgd', attn_weights, value_head, preferred_element_typ...  8.96 us
    dot_general x1, matrix products, per_device(): jnp.dot(attended, lax.all_gather(out_weight, 'dp', axis=1, tiled=True), p...  3.3 us
    unnamed x7, local copies, waits for them, and re-layouts  3.2 us
  transfers between devices with their start and end apart: 1, of which 0 were waited for; matrix products, arithmetic and copies ran while one was open for 37% of the time, Pallas kernels for 0%

commit v1 on v0

--- a/solution.py
+++ b/solution.py
@@ -1,16 +1,26 @@
+import functools
+
 import jax
 import jax.numpy as jnp
+import numpy as np
 from jax import lax
+from jax.experimental import pallas as pl
+from jax.experimental.pallas import tpu as pltpu
 from jax.sharding import PartitionSpec as P
 
 QH = 16
 KVH = 4
 HEAD = 64
 GRID_W = 64
+GROUP = QH // KVH
+BLOCK = GROUP * HEAD
 
 
 EPSILON = 1e-06
 ROTARY_BASE = 10000.0
+
+F32 = jnp.float32
+BF16 = jnp.bfloat16
 
 
 def rotate(vectors, positions, width):
@@ -54,7 +64,7 @@
     return exponent / jnp.sum(exponent, axis=-1, keepdims=True)
 
 
-def per_device(queries, keys, values, query_gain, key_gain, out_weight, out_gain):
+def per_device_general(queries, keys, values, query_gain, key_gain, out_weight, out_gain):
     sp_count = lax.axis_size("sp")
     tokens_here = queries.shape[1]
     seq_len = tokens_here * sp_count
@@ -101,9 +111,373 @@
     return normed.astype(jnp.bfloat16)[None]
 
 
+def position_tables(seq_len):
+    width = HEAD // 2
+    frequency = np.float32(ROTARY_BASE) ** (
+        -np.arange(0, width, 2, dtype=np.float32) / np.float32(width)
+    )
+    position = np.arange(seq_len)
+    parts = []
+    for coordinate in (position // GRID_W, position % GRID_W):
+        angles = coordinate.astype(np.float32)[:, None] * frequency[None, :]
+        parts += [angles, angles]
+    angles = np.concatenate(parts * 2, axis=1).astype(np.float64)
+    return np.stack([np.cos(angles), np.sin(angles)]).astype(np.float32)
+
+
+def dot(a, b):
+    return jnp.dot(a, b, preferred_element_type=F32)
+
+
+def kernel(
+    sp, dp,
+    q_ref, k_ref, v_ref, qg_ref, kg_ref, w_ref, og_ref, table_ref,
+    out_ref,
+    q_raw, q_rot, k_all, v_all, k_rot, tables, w_all, gains,
+    swap_mat, ones_mat, expo, peak, total, att, proj,
+    local_sem, kv_send, kv_recv, w_send, w_recv,
+):
+    tokens = q_raw.shape[0]
+    depth = w_ref.shape[0]
+    half = depth // 2
+    me = lax.axis_index("sp")
+    here = lax.axis_index("dp")
+    mate = here + 1 - 2 * (here % 2)
+    flip_x = 2 - 4 * ((here // 2) % 2)
+    flip_y = 4 - 8 * ((here // 4) % 2)
+    dev_x = here + flip_x
+    dev_y = here + flip_y
+    dev_d = here + flip_x + flip_y
+
+    barrier = pltpu.get_barrier_semaphore()
+    has_left = me > 0
+    has_right = me < sp - 1
+
+    for other in (mate, dev_x, dev_y):
+        pl.semaphore_signal(barrier, inc=1, device_id={"dp": other})
+
+    @pl.when(has_left)
+    def _():
+        pl.semaphore_signal(barrier, inc=1, device_id={"sp": me - 1})
+
+    @pl.when(has_right)
+    def _():
+        pl.semaphore_signal(barrier, inc=1, device_id={"sp": me + 1})
+
+    locals_ = [
+        pltpu.make_async_copy(q_ref, q_raw, local_sem.at[0]),
+        pltpu.make_async_copy(table_ref, tables, local_sem.at[1]),
+        pltpu.make_async_copy(k_ref, k_all.at[pl.ds(me * tokens, tokens)], local_sem.at[2]),
+        pltpu.make_async_copy(v_ref, v_all.at[pl.ds(me * tokens, tokens)], local_sem.at[3]),
+        pltpu.make_async_copy(w_ref, w_all.at[here], local_sem.at[4]),
+    ]
+    for copy in locals_:
+        copy.start()
+
+    pl.semaphore_wait(barrier, 3 + jnp.minimum(me, 1) + jnp.minimum(sp - 1 - me, 1))
+
+    def kv_copies(way, step):
+        block = me - step if way == 0 else me + step
+        target = me + 1 if way == 0 else me - 1
+        rows = pl.ds(block * tokens, tokens)
+        copies = []
+        for i, (own, every) in enumerate(((k_ref, k_all), (v_ref, v_all))):
+            copies.append(
+                pltpu.make_async_remote_copy(
+                    src_ref=own if step == 0 else every.at[rows],
+                    dst_ref=every.at[rows],
+                    send_sem=kv_send.at[way, step, i],
+                    recv_sem=kv_recv.at[way, step, i],
+                    device_id={"sp": target},
+                )
+            )
+        return copies
+
+    def kv_sends(way, step):
+        if way == 0:
+            return jnp.logical_and(has_right, me - step >= 0)
+        return jnp.logical_and(has_left, me + step < sp)
+
+    def kv_start(step):
+        for way in (0, 1):
+            @pl.when(kv_sends(way, step))
+            def _(way=way):
+                for copy in kv_copies(way, step):
+                    copy.start()
+
+    def kv_wait_recv(step):
+        for way in (0, 1):
+            source = me - 1 - step if way == 0 else me + 1 + step
+            arrives = source >= 0 if way == 0 else source < sp
+
+            @pl.when(arrives)
+            def _(way=way, source=source):
+                rows = pl.ds(source * tokens, tokens)
+                for i, every in enumerate((k_all, v_all)):
+                    pltpu.make_async_remote_copy(
+                        src_ref=every.at[rows],
+                        dst_ref=every.at[rows],
+                        send_sem=kv_send.at[way, step, i],
+                        recv_sem=kv_recv.at[way, step, i],
+                        device_id={"sp": me},
+                    ).wait_recv()
+
+    kv_start(0)
+
+    top, bottom, whole = (0, half), (half, half), (0, depth)
+
+    def w_copy(index, shard, rows, target, own=False):
+        window = pl.ds(rows[0], rows[1])
+        return pltpu.make_async_remote_copy(
+            src_ref=w_ref.at[window] if own else w_all.at[shard, window],
+            dst_ref=w_all.at[shard, window],
+            send_sem=w_send.at[index],
+            recv_sem=w_recv.at[index],
+            device_id={"dp": target},
+        )
+
+    def w_wait(index, shard, rows):
+        w_copy(index, shard, rows, mate).wait_recv()
+
+    sent = [
+        w_copy(0, here, bottom, dev_x, own=True),
+        w_copy(2, here, top, dev_y, own=True),
+        w_copy(1, here, top, dev_x, own=True),
+        w_copy(3, here, bottom, dev_y, own=True),
+        w_copy(6, here, whole, mate, own=True),
+    ]
+    for copy in sent:
+        copy.start()
+
+    def w_forward(index, shard, rows, target):
+        copy = w_copy(index, shard, rows, target)
+        copy.start()
+        sent.append(copy)
+
+    row_id = lax.broadcasted_iota(jnp.int32, (BLOCK, BLOCK), 0)
+    col_id = lax.broadcasted_iota(jnp.int32, (BLOCK, BLOCK), 1)
+    quarter = HEAD // 4
+    second = (col_id & (HEAD // 2 - 1)) >= quarter
+    partner_col = jnp.where(second, col_id - quarter, col_id + quarter)
+    hit = row_id == partner_col
+    swap_mat[...] = jnp.where(hit, jnp.where(second, 1.0, -1.0), 0.0).astype(BF16)
+    ones_mat[...] = jnp.where((row_id // HEAD) == (col_id // HEAD), 1.0, 0.0).astype(BF16)
+    spread = jnp.where(
+        row_id[:HEAD] == (col_id[:HEAD] & (HEAD - 1)), 1.0, 0.0
+    ).astype(BF16)
+    spread_swapped = jnp.where(
+        row_id[:HEAD] == (partner_col[:HEAD] & (HEAD - 1)), 1.0, 0.0
+    ).astype(BF16)
+    for i, gain_ref in enumerate((qg_ref, kg_ref)):
+        gain = jnp.broadcast_to(gain_ref[...], (16, HEAD))
+        first = gain.astype(BF16)
+        rest = gain - first.astype(F32)
+        mid = rest.astype(BF16)
+        low = (rest - mid.astype(F32)).astype(BF16)
+        for j, matrix in enumerate((spread, spread_swapped)):
+            gains[2 * i + j] = (dot(first, matrix) + dot(mid, matrix)) + dot(low, matrix)
+
+    lane_head = lax.broadcasted_iota(jnp.int32, (1, BLOCK), 1) // HEAD
+    masks = [jnp.where(lane_head == p, 1.0, 0.0) for p in range(GROUP)]
+
+    def turned(x, rows, which, scale):
+        xf = x.astype(F32)
+        square = xf * xf
+        high = square.astype(BF16)
+        low = (square - high.astype(F32)).astype(BF16)
+        ones = ones_mat[...]
+        mean = (dot(high, ones) + dot(low, ones)) * (1.0 / HEAD)
+        inverse = lax.rsqrt(mean + EPSILON) * scale
+        swapped = dot(x, swap_mat[...])
+        cosines = tables[0, rows, :]
+        sines = tables[1, rows, :]
+        cosines = jnp.concatenate([cosines, cosines], axis=1) * gains[2 * which, 0:1, :]
+        sines = jnp.concatenate([sines, sines], axis=1) * gains[2 * which + 1, 0:1, :]
+        return ((xf * cosines + swapped * sines) * inverse).astype(BF16)
+
+    locals_[0].wait()
+    locals_[1].wait()
+    own_rows = pl.ds(pl.multiple_of(me * tokens, 64), tokens)
+    for b in range(KVH):
+        columns = slice(b * BLOCK, (b + 1) * BLOCK)
+        q_rot[:, columns] = turned(q_raw[:, columns], own_rows, 0, HEAD ** (-0.5))
+
+    pairs = sp // 2
+    mine = me // 2
+
+    def attend(turn):
+        span = 2 * tokens
+        pair = lax.rem(mine + turn, pairs)
+        rows = pl.ds(pl.multiple_of(pair * span, 128), span)
+        k_rot[...] = turned(k_all[rows, :], rows, 1, 1.0)
+        before = [pl.ds(pl.multiple_of(lax.rem(mine + t, pairs) * span, 128), span) for t in range(turn)]
+
+        def one(b, carry):
+            columns = pl.ds(pl.multiple_of(b * BLOCK, BLOCK), BLOCK)
+            pick = jnp.where(row_id == b * HEAD + (col_id & (HEAD - 1)), 1.0, 0.0).astype(BF16)
+            key = dot(k_rot[...], pick).astype(BF16)
+            query = q_rot[:, columns]
+            if turn == pairs - 1:
+                value = dot(v_all[rows, :], pick).astype(BF16)
+                olds = [dot(v_all[r, :], pick).astype(BF16) for r in before]
+            out = 0.0
+            for p in range(GROUP):
+                mask = masks[p]
+                head = b * GROUP + p
+                scores = lax.dot_general(
+                    query * mask.astype(BF16), key, (((1,), (1,)), ((), ())),
+                    preferred_element_type=F32,
+                )
+                high = jnp.max(scores, axis=1, keepdims=True)
+                if turn < pairs - 1:
+                    weights = jnp.exp(scores - high)
+                    expo[turn, head] = weights
+                    peak[turn, head] = high
+                    total[turn, head] = jnp.sum(weights, axis=1, keepdims=True)
+                    continue
+                for t in range(turn):
+                    high = jnp.maximum(high, peak[t, head])
+                weights = jnp.exp(scores - high)
+                norm = jnp.sum(weights, axis=1, keepdims=True)
+                keeps = [jnp.exp(peak[t, head] - high) for t in range(turn)]
+                for t in range(turn):
+                    norm = norm + total[t, head] * keeps[t]
+                inverse = 1.0 / norm
+                product = dot((weights * inverse).astype(BF16), value)
+                for t in range(turn):
+                    old = expo[t, head] * (keeps[t] * inverse)
+                    product = product + dot(old.astype(BF16), olds[t])
+                out = out + product * mask
+            if turn == pairs - 1:
+                att[:, columns] = out.astype(BF16)
+            return carry
+
+        lax.fori_loop(0, KVH, one, 0)
+
+    locals_[2].wait()
+    locals_[3].wait()
+
+    kv_wait_recv(0)
+    if sp > 2:
+        kv_start(1)
+
+    w_wait(0, dev_x, bottom)
+    w_forward(5, dev_x, bottom, dev_y)
+    w_wait(2, dev_y, top)
+    w_forward(4, dev_y, top, dev_x)
+    w_forward(7, dev_x, bottom, mate)
+    w_forward(9, dev_y, top, mate)
+
+    attend(0)
+    for step in range(1, sp - 1):
+        kv_wait_recv(step)
+        if step < sp - 2:
+            kv_start(step + 1)
+    w_wait(1, dev_x, top)
+    w_forward(8, dev_x, top, mate)
+    w_wait(3, dev_y, bottom)
+    w_forward(10, dev_y, bottom, mate)
+    for turn in range(1, pairs):
+        attend(turn)
+
+    columns_each = w_ref.shape[1]
+
+    def project(shard, squares):
+        columns = pl.ds(pl.multiple_of(shard * columns_each, columns_each), columns_each)
+        result = dot(att[...], w_all[shard])
+        proj[:, columns] = result
+        return squares + jnp.sum(result * result, axis=1, keepdims=True)
+
+    mate_x, mate_y, mate_d = mate + flip_x, mate + flip_y, mate + flip_x + flip_y
+    locals_[4].wait()
+    squares = project(here, jnp.zeros((tokens, 1), F32))
+    w_wait(6, mate, whole)
+    squares = project(mate, squares)
+    squares = project(dev_x, squares)
+    squares = project(dev_y, squares)
+    w_wait(7, mate_x, bottom)
+    w_wait(8, mate_x, top)
+    squares = project(mate_x, squares)
+    w_wait(9, mate_y, top)
+    w_wait(10, mate_y, bottom)
+    squares = project(mate_y, squares)
+    w_wait(4, dev_d, top)
+    w_forward(11, dev_d, top, mate)
+    w_wait(5, dev_d, bottom)
+    w_forward(12, dev_d, bottom, mate)
+    squares = project(dev_d, squares)
+    w_wait(11, mate_d, top)
+    w_wait(12, mate_d, bottom)
+    squares = project(mate_d, squares)
+
+    inverse = lax.rsqrt(squares * (1.0 / (columns_each * dp)) + EPSILON)
+    for j in range(dp):
+        columns = slice(j * columns_each, (j + 1) * columns_each)
+        out_ref[:, columns] = (proj[:, columns] * inverse * og_ref[:, columns]).astype(BF16)
+
+    for copy in sent:
+        copy.wait_send()
+    for step in range(sp - 1):
+        for way in (0, 1):
+            @pl.when(kv_sends(way, step))
+            def _(way=way, step=step):
+                for copy in kv_copies(way, step):
+                    copy.wait_send()
+
+
+def per_device_fused(sp, dp, queries, keys, values, query_gain, key_gain, out_weight, out_gain):
+    tokens = queries.shape[1]
+    depth, columns = out_weight.shape
+    hidden = queries.shape[2]
+    kv_width = keys.shape[2]
+    seq_len = tokens * sp
+    hbm_spec = pl.BlockSpec(memory_space=pltpu.HBM)
+    vmem_spec = pl.BlockSpec(memory_space=pltpu.VMEM)
+    result = pl.pallas_call(
+        functools.partial(kernel, sp, dp),
+        out_shape=jax.ShapeDtypeStruct((tokens, columns * dp), BF16),
+        in_specs=[hbm_spec] * 3 + [vmem_spec] * 2 + [hbm_spec, vmem_spec, hbm_spec],
+        out_specs=vmem_spec,
+        scratch_shapes=[
+            pltpu.VMEM((tokens, hidden), BF16),
+            pltpu.VMEM((tokens, hidden), BF16),
+            pltpu.VMEM((seq_len, kv_width), BF16),
+            pltpu.VMEM((seq_len, kv_width), BF16),
+            pltpu.VMEM((2 * tokens, kv_width), BF16),
+            pltpu.VMEM((2, seq_len, 2 * HEAD), F32),
+            pltpu.VMEM((dp, depth, columns), BF16),
+            pltpu.VMEM((4, 16, BLOCK), F32),
+            pltpu.VMEM((BLOCK, BLOCK), BF16),
+            pltpu.VMEM((BLOCK, BLOCK), BF16),
+            pltpu.VMEM((max(sp // 2 - 1, 1), QH, tokens, 2 * tokens), F32),
+            pltpu.VMEM((max(sp // 2 - 1, 1), QH, tokens, 1), F32),
+            pltpu.VMEM((max(sp // 2 - 1, 1), QH, tokens, 1), F32),
+            pltpu.VMEM((tokens, hidden), BF16),
+            pltpu.VMEM((tokens, columns * dp), F32),
+            pltpu.SemaphoreType.DMA((5,)),
+            pltpu.SemaphoreType.DMA((2, sp - 1, 2)),
+            pltpu.SemaphoreType.DMA((2, sp - 1, 2)),
+            pltpu.SemaphoreType.DMA((13,)),
+            pltpu.SemaphoreType.DMA((13,)),
+        ],
+        compiler_params=pltpu.CompilerParams(
+            collective_id=0, has_side_effects=True, vmem_limit_bytes=48 * 1024 * 1024
+        ),
+    )(
+        queries[0], keys[0], values[0], query_gain[None], key_gain[None],
+        out_weight, out_gain[None], jnp.asarray(position_tables(seq_len)),
+    )
+    return result[None]
+
+
 def solution(mesh):
+    sp, dp = mesh.shape["sp"], mesh.shape["dp"]
+    if dp == 8 and sp >= 2 and sp % 2 == 0 and sp <= 4:
+        body = functools.partial(per_device_fused, sp, dp)
+    else:
+        body = per_device_general
     return jax.shard_map(
-        per_device,
+        body,
         mesh=mesh,
         in_specs=(
             P("dp", "sp", None),

time: 64 us -> 43.1 us (0.67)
  the two profiles are of different devices: /device:TPU:0 before, /device:TPU:1 now
where the time goes in v1:
time: 43.1 us; the launch traced here: 42.8 us
  Pallas kernels  36.2 us (84%)
  local copies, waits for them, and re-layouts  6.53 us (15%)
    pallas_call x1, Pallas kernels, per_device_fused(): pl.pallas_call(functools.partial(kernel, sp, dp), out_shape=jax.ShapeDtyp...  36.2 us
    unnamed x17, local copies, waits for them, and re-layouts  6.53 us

profile of v1, /device:TPU:1, one launch (start us, length us, event | category | flops | bytes accessed | tf_op | source)
XLA Modules:
  0.0 42.8 jit_solution(8806653027615742888)
XLA Ops:
  0.0 0.0 copy-start.5
  0.0 0.0 copy-start.6
  0.0 0.0 copy-start.7
  0.0 0.7 %copy-done.5 = f32[2048]{0:T(1024)S(1)} copy-done((f32[2048]{0:T(1024)S(1)}, f32[2048]{0:T(1024)}, u32[]{:S(2)}) %copy-start.5) | copy-done | bytes 8216
  0.7 0.0 copy-done.6
  0.7 0.0 copy-done.7
  0.7 0.0 copy-start
  0.7 1.1 %copy-done = f32[2,768,128]{2,1,0:T(8,128)S(1)} copy-done((f32[2,768,128]{2,1,0:T(8,128)S(1)}, f32[2,768,128]{2,1,0:T(8,128)}, u32[]{:S(2)}) %copy-start) | copy-done | bytes 786456
  1.8 0.0 copy-start.1
  1.8 1.0 %copy-done.1 = bf16[1024,256]{1,0:T(8,128)(2,1)S(1)} copy-done((bf16[1024,256]{1,0:T(8,128)(2,1)S(1)}, bf16[1024,256]{1,0:T(8,128)(2,1)}, u32[]{:S(2)}) %copy-start.1) | copy-done | bytes 524312
  2.9 0.0 copy-start.2
  2.9 1.0 %copy-done.2 = bf16[1,192,1024]{2,1,0:T(8,128)(2,1)S(1)} copy-done((bf16[1,192,1024]{2,1,0:T(8,128)(2,1)S(1)}, bf16[1,192,1024]{2,1,0:T(8,128)(2,1)}, u32[]{:S(2)}) %copy-start.2) | copy-done | bytes 393240
  3.9 0.0 copy-start.3
  3.9 0.9 %copy-done.3 = bf16[1,192,256]{2,1,0:T(8,128)(2,1)S(1)} copy-done((bf16[1,192,256]{2,1,0:T(8,128)(2,1)S(1)}, bf16[1,192,256]{2,1,0:T(8,128)(2,1)}, u32[]{:S(2)}) %copy-start.3) | copy-done | bytes 98328
  4.8 0.0 copy-start.4
  4.8 0.9 %copy-done.4 = bf16[1,192,256]{2,1,0:T(8,128)(2,1)S(1)} copy-done((bf16[1,192,256]{2,1,0:T(8,128)(2,1)S(1)}, bf16[1,192,256]{2,1,0:T(8,128)(2,1)}, u32[]{:S(2)}) %copy-start.4) | copy-done | bytes 98328
  5.7 36.2 %shard_map.82 = bf16[192,2048]{1,0:T(8,128)(2,1)S(1)} custom-call(bf16[192,1024]{1,0:T(8,128)(2,1)S(1)} %bitcast.8, bf16[192,256]{1,0:T(8,128)(2,1)S(1)} %bitcast.9, bf16[192,256]{1,0:T(8,128)(2,1)S(1)} %bitcast.10, f32[1,64]{1,0:T(1,128)S(1)} %bitcast.12, f32[1,64]{1,0:T(1,128)S(1)} %bitcast.13, bf16[1024,256]{1,0:T(8,128)(2,1)S(1)} %copy-done.1, ...), custom_call_target="tpu_custom_call" | custom-call | tf_op jit(solution)/shard_map/pallas_call | solution.py:436
  41.9 0.9 %copy.10 = bf16[1,192,2048]{2,1,0:T(8,128)(2,1)} copy(bf16[1,192,2048]{2,1,0:T(8,128)(2,1)S(1)} %bitcast.7) | data formatting | bytes 1572864
Async XLA Ops:
  0.0 0.7 %copy-start.5 = (f32[2048]{0:T(1024)S(1)}, f32[2048]{0:T(1024)}, u32[]{:S(2)}) copy-start(f32[2048]{0:T(1024)} %param.14) | copy-start | bytes 24580
  0.0 0.7 %copy-start.6 = (f32[64]{0:T(128)S(1)}, f32[64]{0:T(128)}, u32[]{:S(2)}) copy-start(f32[64]{0:T(128)} %param.11) | copy-start | bytes 772
  0.0 0.7 %copy-start.7 = (f32[64]{0:T(128)S(1)}, f32[64]{0:T(128)}, u32[]{:S(2)}) copy-start(f32[64]{0:T(128)} %param.12) | copy-start | bytes 772
  0.7 1.1 %copy-start = (f32[2,768,128]{2,1,0:T(8,128)S(1)}, f32[2,768,128]{2,1,0:T(8,128)}, u32[]{:S(2)}) copy-start(f32[2,768,128]{2,1,0:T(8,128)} %constant.2.clone.table_ref) | copy-start | bytes 2359300
  1.8 1.0 %copy-start.1 = (bf16[1024,256]{1,0:T(8,128)(2,1)S(1)}, bf16[1024,256]{1,0:T(8,128)(2,1)}, u32[]{:S(2)}) copy-start(bf16[1024,256]{1,0:T(8,128)(2,1)} %w_ref.1) | copy-start | bytes 1572868
  2.9 1.0 %copy-start.2 = (bf16[1,192,1024]{2,1,0:T(8,128)(2,1)S(1)}, bf16[1,192,1024]{2,1,0:T(8,128)(2,1)}, u32[]{:S(2)}) copy-start(bf16[1,192,1024]{2,1,0:T(8,128)(2,1)} %param.8) | copy-start | bytes 1179652
  3.9 0.9 %copy-start.3 = (bf16[1,192,256]{2,1,0:T(8,128)(2,1)S(1)}, bf16[1,192,256]{2,1,0:T(8,128)(2,1)}, u32[]{:S(2)}) copy-start(bf16[1,192,256]{2,1,0:T(8,128)(2,1)} %param.9) | copy-start | bytes 294916
  4.8 0.9 %copy-start.4 = (bf16[1,192,256]{2,1,0:T(8,128)(2,1)S(1)}, bf16[1,192,256]{2,1,0:T(8,128)(2,1)}, u32[]{:S(2)}) copy-start(bf16[1,192,256]{2,1,0:T(8,128)(2,1)} %param.10) | copy-start | bytes 294916

commit v2 on v1

--- a/solution.py
+++ b/solution.py
@@ -129,12 +129,17 @@
     return jnp.dot(a, b, preferred_element_type=F32)
 
 
+def cross(a, b):
+    return lax.dot_general(a, b, (((1,), (1,)), ((), ())), preferred_element_type=F32)
+
+
 def kernel(
     sp, dp,
     q_ref, k_ref, v_ref, qg_ref, kg_ref, w_ref, og_ref, table_ref,
     out_ref,
     q_raw, q_rot, k_all, v_all, k_rot, tables, w_all, gains,
-    swap_mat, ones_mat, expo, peak, total, att, proj,
+    swap_mat, ones_mat, place_mat, back_mat, v_turned,
+    expo, peak, total, att, proj,
     local_sem, kv_send, kv_recv, w_send, w_recv,
 ):
     tokens = q_raw.shape[0]
@@ -305,51 +310,56 @@
     pairs = sp // 2
     mine = me // 2
 
+    eye = jnp.where(row_id == col_id, 1.0, 0.0).astype(BF16)
+    wide = GROUP * tokens
+    lane = lax.broadcasted_iota(jnp.int32, (BLOCK, wide), 1)
+    line = lax.broadcasted_iota(jnp.int32, (BLOCK, wide), 0) // HEAD * tokens
+    inside = jnp.logical_and(lane >= line, lane < line + tokens)
+    place_mat[...] = jnp.where(inside, 1.0, 0.0).astype(BF16)
+    lane = lax.broadcasted_iota(jnp.int32, (tokens, wide), 1)
+    line = lax.broadcasted_iota(jnp.int32, (tokens, wide), 0)
+    hit = lane == line
+    for p in range(1, GROUP):
+        hit = jnp.logical_or(hit, lane == line + p * tokens)
+    back_mat[...] = jnp.where(hit, 1.0, 0.0).astype(BF16)
+
     def attend(turn):
         span = 2 * tokens
         pair = lax.rem(mine + turn, pairs)
         rows = pl.ds(pl.multiple_of(pair * span, 128), span)
         k_rot[...] = turned(k_all[rows, :], rows, 1, 1.0)
-        before = [pl.ds(pl.multiple_of(lax.rem(mine + t, pairs) * span, 128), span) for t in range(turn)]
+        v_turned[turn] = cross(eye, v_all[rows, :]).astype(BF16)
 
         def one(b, carry):
             columns = pl.ds(pl.multiple_of(b * BLOCK, BLOCK), BLOCK)
+            value_rows = pl.ds(pl.multiple_of(b * HEAD, HEAD), HEAD)
             pick = jnp.where(row_id == b * HEAD + (col_id & (HEAD - 1)), 1.0, 0.0).astype(BF16)
             key = dot(k_rot[...], pick).astype(BF16)
             query = q_rot[:, columns]
-            if turn == pairs - 1:
-                value = dot(v_all[rows, :], pick).astype(BF16)
-                olds = [dot(v_all[r, :], pick).astype(BF16) for r in before]
-            out = 0.0
-            for p in range(GROUP):
-                mask = masks[p]
-                head = b * GROUP + p
-                scores = lax.dot_general(
-                    query * mask.astype(BF16), key, (((1,), (1,)), ((), ())),
-                    preferred_element_type=F32,
-                )
-                high = jnp.max(scores, axis=1, keepdims=True)
-                if turn < pairs - 1:
-                    weights = jnp.exp(scores - high)
-                    expo[turn, head] = weights
-                    peak[turn, head] = high
-                    total[turn, head] = jnp.sum(weights, axis=1, keepdims=True)
-                    continue
-                for t in range(turn):
-                    high = jnp.maximum(high, peak[t, head])
+            query = jnp.concatenate([query * mask.astype(BF16) for mask in masks], axis=0)
+            scores = cross(key, query)
+            high = jnp.max(scores, axis=0, keepdims=True)
+            if turn < pairs - 1:
                 weights = jnp.exp(scores - high)
-                norm = jnp.sum(weights, axis=1, keepdims=True)
-                keeps = [jnp.exp(peak[t, head] - high) for t in range(turn)]
-                for t in range(turn):
-                    norm = norm + total[t, head] * keeps[t]
-                inverse = 1.0 / norm
-                product = dot((weights * inverse).astype(BF16), value)
-                for t in range(turn):
-                    old = expo[t, head] * (keeps[t] * inverse)
-                    product = product + dot(old.astype(BF16), olds[t])
-                out = out + product * mask
-            if turn == pairs - 1:
-                att[:, columns] = out.astype(BF16)
+                expo[turn, b] = weights
+                peak[turn, b] = high
+                total[turn, b] = jnp.sum(weights, axis=0, keepdims=True)
+                return carry
+            for t in range(turn):
+                high = jnp.maximum(high, peak[t, b])
+            weights = jnp.exp(scores - high)
+            norm = jnp.sum(weights, axis=0, keepdims=True)
+            keeps = [jnp.exp(peak[t, b] - high) for t in range(turn)]
+            for t in range(turn):
+                norm = norm + total[t, b] * keeps[t]
+            inverse = 1.0 / norm
+            product = dot(v_turned[turn, value_rows, :], (weights * inverse).astype(BF16))
+            for t in range(turn):
+                old = expo[t, b] * (keeps[t] * inverse)
+                product = product + dot(v_turned[t, value_rows, :], old.astype(BF16))
+            product = product.astype(BF16)
+            placed = jnp.concatenate([product] * GROUP, axis=0) * place_mat[...]
+            att[:, columns] = cross(back_mat[...], placed).astype(BF16)
             return carry
 
         lax.fori_loop(0, KVH, one, 0)
@@ -449,9 +459,12 @@
             pltpu.VMEM((4, 16, BLOCK), F32),
             pltpu.VMEM((BLOCK, BLOCK), BF16),
             pltpu.VMEM((BLOCK, BLOCK), BF16),
-            pltpu.VMEM((max(sp // 2 - 1, 1), QH, tokens, 2 * tokens), F32),
-            pltpu.VMEM((max(sp // 2 - 1, 1), QH, tokens, 1), F32),
-            pltpu.VMEM((max(sp // 2 - 1, 1), QH, tokens, 1), F32),
+            pltpu.VMEM((BLOCK, GROUP * tokens), BF16),
+            pltpu.VMEM((tokens, GROUP * tokens), BF16),
+            pltpu.VMEM((sp // 2, kv_width, 2 * tokens), BF16),
+            pltpu.VMEM((max(sp // 2 - 1, 1), KVH, 2 * tokens, GROUP * tokens), F32),
+            pltpu.VMEM((max(sp // 2 - 1, 1), KVH, 1, GROUP * tokens), F32),
+            pltpu.VMEM((max(sp // 2 - 1, 1), KVH, 1, GROUP * tokens), F32),
             pltpu.VMEM((tokens, hidden), BF16),
             pltpu.VMEM((tokens, columns * dp), F32),
             pltpu.SemaphoreType.DMA((5,)),
@@ -461,7 +474,7 @@
             pltpu.SemaphoreType.DMA((13,)),
         ],
         compiler_params=pltpu.CompilerParams(
-            collective_id=0, has_side_effects=True, vmem_limit_bytes=48 * 1024 * 1024
+            collective_id=0, has_side_effects=True, vmem_limit_bytes=67043328
         ),
     )(
         queries[0], keys[0], values[0], query_gain[None], key_gain[None],

time: 43.1 us -> 34.1 us (0.79)
  local copies, waits for them, and re-layouts: 6.53 us -> 2.09 us
  Pallas kernels: 36.2 us -> 31.8 us
    unnamed x17 -> x1, local copies, waits for them, and re-layouts: 6.53 us -> 2.09 us
    pallas_call x1, Pallas kernels: 36.2 us -> 31.8 us  [per_device_fused(): pl.pallas_call(functools.partial(kernel, sp, dp), out_shape=jax.ShapeDtyp...]
where the time goes in v2:
time: 34.1 us; the launch traced here: 33.9 us
  Pallas kernels  31.8 us (93%)
  local copies, waits for them, and re-layouts  2.09 us (6%)
    pallas_call x1, Pallas kernels, per_device_fused(): pl.pallas_call(functools.partial(kernel, sp, dp), out_shape=jax.ShapeDtyp...  31.8 us
    unnamed x1, local copies, waits for them, and re-layouts  2.09 us

profile of v2, /device:TPU:1, one launch (start us, length us, event | category | flops | bytes accessed | tf_op | source)
XLA Modules:
  0.0 33.9 jit_solution(9472230005370957615)
XLA Ops:
  0.0 31.8 %shard_map.82 = bf16[192,2048]{1,0:T(8,128)(2,1)} custom-call(bf16[192,1024]{1,0:T(8,128)(2,1)} %bitcast.8, bf16[192,256]{1,0:T(8,128)(2,1)} %bitcast.9, bf16[192,256]{1,0:T(8,128)(2,1)} %bitcast.10, f32[1,64]{1,0:T(1,128)} %bitcast.12, f32[1,64]{1,0:T(1,128)} %bitcast.13, bf16[1024,256]{1,0:T(8,128)(2,1)} %w_ref.1, f32[1,2048]{1,0:T(1,128)} %bitcast.11, ...), custom_call_target="tpu_custom_call" | custom-call | tf_op jit(solution)/shard_map/pallas_call | solution.py:446
  31.8 2.1 %copy.10 = bf16[1,192,2048]{2,1,0:T(8,128)(2,1)} copy(bf16[1,192,2048]{2,1,0:T(8,128)(2,1)} %bitcast.7) | data formatting | bytes 1572864

commit v3 on v2

--- a/solution.py
+++ b/solution.py
@@ -13,6 +13,7 @@
 HEAD = 64
 GRID_W = 64
 GROUP = QH // KVH
+HALVES = 2
 BLOCK = GROUP * HEAD
 
 
@@ -137,7 +138,7 @@
     sp, dp,
     q_ref, k_ref, v_ref, qg_ref, kg_ref, w_ref, og_ref, table_ref,
     out_ref,
-    q_raw, q_rot, k_all, v_all, k_rot, tables, w_all, gains,
+    q_raw, q_rot, k_all, v_all, tables, w_all, gains,
     swap_mat, ones_mat, place_mat, back_mat, v_turned,
     expo, peak, total, att, proj,
     local_sem, kv_send, kv_recv, w_send, w_recv,
@@ -181,18 +182,21 @@
 
     pl.semaphore_wait(barrier, 3 + jnp.minimum(me, 1) + jnp.minimum(sp - 1 - me, 1))
 
-    def kv_copies(way, step):
+    part = k_ref.shape[1] // HALVES
+
+    def kv_copies(way, step, side):
         block = me - step if way == 0 else me + step
         target = me + 1 if way == 0 else me - 1
         rows = pl.ds(block * tokens, tokens)
+        columns = pl.ds(side * part, part)
         copies = []
         for i, (own, every) in enumerate(((k_ref, k_all), (v_ref, v_all))):
             copies.append(
                 pltpu.make_async_remote_copy(
-                    src_ref=own if step == 0 else every.at[rows],
-                    dst_ref=every.at[rows],
-                    send_sem=kv_send.at[way, step, i],
-                    recv_sem=kv_recv.at[way, step, i],
+                    src_ref=own.at[:, columns] if step == 0 else every.at[rows, columns],
+                    dst_ref=every.at[rows, columns],
+                    send_sem=kv_send.at[way, step, side, i],
+                    recv_sem=kv_recv.at[way, step, side, i],
                     device_id={"sp": target},
                 )
             )
@@ -203,31 +207,35 @@
             return jnp.logical_and(has_right, me - step >= 0)
         return jnp.logical_and(has_left, me + step < sp)
 
-    def kv_start(step):
+    def kv_start(step, side):
+        if step >= sp - 1:
+            return
         for way in (0, 1):
             @pl.when(kv_sends(way, step))
             def _(way=way):
-                for copy in kv_copies(way, step):
+                for copy in kv_copies(way, step, side):
                     copy.start()
 
-    def kv_wait_recv(step):
+    def kv_arrive(step, side):
         for way in (0, 1):
             source = me - 1 - step if way == 0 else me + 1 + step
             arrives = source >= 0 if way == 0 else source < sp
 
             @pl.when(arrives)
             def _(way=way, source=source):
-                rows = pl.ds(source * tokens, tokens)
+                window = (pl.ds(source * tokens, tokens), pl.ds(side * part, part))
                 for i, every in enumerate((k_all, v_all)):
                     pltpu.make_async_remote_copy(
-                        src_ref=every.at[rows],
-                        dst_ref=every.at[rows],
-                        send_sem=kv_send.at[way, step, i],
-                        recv_sem=kv_recv.at[way, step, i],
+                        src_ref=every.at[window],
+                        dst_ref=every.at[window],
+                        send_sem=kv_send.at[way, step, side, i],
+                        recv_sem=kv_recv.at[way, step, side, i],
                         device_id={"sp": me},
                     ).wait_recv()
-
-    kv_start(0)
+        kv_start(step + 1, side)
+
+    for side in range(HALVES):
+        kv_start(0, side)
 
     top, bottom, whole = (0, half), (half, half), (0, depth)
 
@@ -290,14 +298,18 @@
         square = xf * xf
         high = square.astype(BF16)
         low = (square - high.astype(F32)).astype(BF16)
-        ones = ones_mat[...]
+        size = x.shape[1]
+        ones = ones_mat[:size, :size]
         mean = (dot(high, ones) + dot(low, ones)) * (1.0 / HEAD)
         inverse = lax.rsqrt(mean + EPSILON) * scale
-        swapped = dot(x, swap_mat[...])
+        swapped = dot(x, swap_mat[:size, :size])
         cosines = tables[0, rows, :]
         sines = tables[1, rows, :]
-        cosines = jnp.concatenate([cosines, cosines], axis=1) * gains[2 * which, 0:1, :]
-        sines = jnp.concatenate([sines, sines], axis=1) * gains[2 * which + 1, 0:1, :]
+        if size > 2 * HEAD:
+            cosines = jnp.concatenate([cosines, cosines], axis=1)
+            sines = jnp.concatenate([sines, sines], axis=1)
+        cosines = cosines * gains[2 * which, 0:1, :size]
+        sines = sines * gains[2 * which + 1, 0:1, :size]
         return ((xf * cosines + swapped * sines) * inverse).astype(BF16)
 
     locals_[0].wait()
@@ -323,18 +335,21 @@
         hit = jnp.logical_or(hit, lane == line + p * tokens)
     back_mat[...] = jnp.where(hit, 1.0, 0.0).astype(BF16)
 
-    def attend(turn):
+    def attend(turn, side):
         span = 2 * tokens
         pair = lax.rem(mine + turn, pairs)
         rows = pl.ds(pl.multiple_of(pair * span, 128), span)
-        k_rot[...] = turned(k_all[rows, :], rows, 1, 1.0)
-        v_turned[turn] = cross(eye, v_all[rows, :]).astype(BF16)
-
-        def one(b, carry):
-            columns = pl.ds(pl.multiple_of(b * BLOCK, BLOCK), BLOCK)
-            value_rows = pl.ds(pl.multiple_of(b * HEAD, HEAD), HEAD)
-            pick = jnp.where(row_id == b * HEAD + (col_id & (HEAD - 1)), 1.0, 0.0).astype(BF16)
-            key = dot(k_rot[...], pick).astype(BF16)
+        lanes = slice(side * part, (side + 1) * part)
+        key_side = turned(k_all[rows, lanes], rows, 1, 1.0)
+        v_turned[turn, lanes, :] = cross(eye[:part, :part], v_all[rows, lanes]).astype(BF16)
+        heads = KVH // HALVES
+
+        def one(b):
+            columns = slice(b * BLOCK, (b + 1) * BLOCK)
+            value_rows = slice(b * HEAD, (b + 1) * HEAD)
+            source = (b - side * heads) * HEAD + (col_id[:part] & (HEAD - 1))
+            pick = jnp.where(row_id[:part] == source, 1.0, 0.0).astype(BF16)
+            key = dot(key_side, pick).astype(BF16)
             query = q_rot[:, columns]
             query = jnp.concatenate([query * mask.astype(BF16) for mask in masks], axis=0)
             scores = cross(key, query)
@@ -344,7 +359,7 @@
                 expo[turn, b] = weights
                 peak[turn, b] = high
                 total[turn, b] = jnp.sum(weights, axis=0, keepdims=True)
-                return carry
+                return
             for t in range(turn):
                 high = jnp.maximum(high, peak[t, b])
             weights = jnp.exp(scores - high)
@@ -360,16 +375,18 @@
             product = product.astype(BF16)
             placed = jnp.concatenate([product] * GROUP, axis=0) * place_mat[...]
             att[:, columns] = cross(back_mat[...], placed).astype(BF16)
-            return carry
-
-        lax.fori_loop(0, KVH, one, 0)
+
+        for b in range(side * heads, (side + 1) * heads):
+            one(b)
 
     locals_[2].wait()
     locals_[3].wait()
 
-    kv_wait_recv(0)
-    if sp > 2:
-        kv_start(1)
+    last = HALVES - 1
+    for side in range(HALVES):
+        kv_arrive(0, side)
+    for side in range(last):
+        attend(0, side)
 
     w_wait(0, dev_x, bottom)
     w_forward(5, dev_x, bottom, dev_y)
@@ -377,18 +394,26 @@
     w_forward(4, dev_y, top, dev_x)
     w_forward(7, dev_x, bottom, mate)
     w_forward(9, dev_y, top, mate)
-
-    attend(0)
-    for step in range(1, sp - 1):
-        kv_wait_recv(step)
-        if step < sp - 2:
-            kv_start(step + 1)
-    w_wait(1, dev_x, top)
-    w_forward(8, dev_x, top, mate)
-    w_wait(3, dev_y, bottom)
-    w_forward(10, dev_y, bottom, mate)
-    for turn in range(1, pairs):
-        attend(turn)
+    for step in range(1, sp - 2):
+        for side in range(HALVES):
+            kv_arrive(step, side)
+
+    attend(0, last)
+    if sp > 2:
+        for side in range(HALVES):
+            kv_arrive(sp - 2, side)
+            if side == last:
+                w_wait(1, dev_x, top)
+                w_forward(8, dev_x, top, mate)
+                w_wait(3, dev_y, bottom)
+                w_forward(10, dev_y, bottom, mate)
+            for turn in range(1, pairs):
+                attend(turn, side)
+    else:
+        w_wait(1, dev_x, top)
+        w_forward(8, dev_x, top, mate)
+        w_wait(3, dev_y, bottom)
+        w_forward(10, dev_y, bottom, mate)
 
     columns_each = w_ref.shape[1]
 
@@ -431,8 +456,9 @@
         for way in (0, 1):
             @pl.when(kv_sends(way, step))
             def _(way=way, step=step):
-                for copy in kv_copies(way, step):
-                    copy.wait_send()
+                for side in range(HALVES):
+                    for copy in kv_copies(way, step, side):
+                        copy.wait_send()
 
 
 def per_device_fused(sp, dp, queries, keys, values, query_gain, key_gain, out_weight, out_gain):
@@ -445,7 +471,7 @@
     vmem_spec = pl.BlockSpec(memory_space=pltpu.VMEM)
     result = pl.pallas_call(
         functools.partial(kernel, sp, dp),
-        out_shape=jax.ShapeDtypeStruct((tokens, columns * dp), BF16),
+        out_shape=pltpu.VMEM((tokens, columns * dp), BF16),
         in_specs=[hbm_spec] * 3 + [vmem_spec] * 2 + [hbm_spec, vmem_spec, hbm_spec],
         out_specs=vmem_spec,
         scratch_shapes=[
@@ -453,7 +479,6 @@
             pltpu.VMEM((tokens, hidden), BF16),
             pltpu.VMEM((seq_len, kv_width), BF16),
             pltpu.VMEM((seq_len, kv_width), BF16),
-            pltpu.VMEM((2 * tokens, kv_width), BF16),
             pltpu.VMEM((2, seq_len, 2 * HEAD), F32),
             pltpu.VMEM((dp, depth, columns), BF16),
             pltpu.VMEM((4, 16, BLOCK), F32),
@@ -468,13 +493,13 @@
             pltpu.VMEM((tokens, hidden), BF16),
             pltpu.VMEM((tokens, columns * dp), F32),
             pltpu.SemaphoreType.DMA((5,)),
-            pltpu.SemaphoreType.DMA((2, sp - 1, 2)),
-            pltpu.SemaphoreType.DMA((2, sp - 1, 2)),
+            pltpu.SemaphoreType.DMA((2, sp - 1, HALVES, 2)),
+            pltpu.SemaphoreType.DMA((2, sp - 1, HALVES, 2)),
             pltpu.SemaphoreType.DMA((13,)),
             pltpu.SemaphoreType.DMA((13,)),
         ],
         compiler_params=pltpu.CompilerParams(
-            collective_id=0, has_side_effects=True, vmem_limit_bytes=67043328
+            collective_id=0, has_side_effects=True, vmem_limit_bytes=66000000
         ),
     )(
         queries[0], keys[0], values[0], query_gain[None], key_gain[None],

time: 34.1 us -> 28.7 us (0.84)
  Pallas kernels: 31.8 us -> 27.6 us
  local copies, waits for them, and re-layouts: 2.09 us -> 0.88 us
    pallas_call x1, Pallas kernels: 31.8 us -> 27.6 us  [per_device_fused(): pl.pallas_call(functools.partial(kernel, sp, dp), out_shape=pltpu.VMEM((t...]
    unnamed x1, local copies, waits for them, and re-layouts: 2.09 us -> 0.88 us
where the time goes in v3:
time: 28.7 us; the launch traced here: 28.5 us
  Pallas kernels  27.6 us (96%)
  local copies, waits for them, and re-layouts  0.88 us (3%)
    pallas_call x1, Pallas kernels, per_device_fused(): pl.pallas_call(functools.partial(kernel, sp, dp), out_shape=pltpu.VMEM((t...  27.6 us
    unnamed x1, local copies, waits for them, and re-layouts  0.88 us

profile of v3, /device:TPU:1, one launch (start us, length us, event | category | flops | bytes accessed | tf_op | source)
XLA Modules:
  0.0 28.5 jit_solution(12243123932610571021)
XLA Ops:
  0.0 27.6 %shard_map.82 = bf16[192,2048]{1,0:T(8,128)(2,1)S(1)} custom-call(bf16[192,1024]{1,0:T(8,128)(2,1)} %bitcast.8, bf16[192,256]{1,0:T(8,128)(2,1)} %bitcast.9, bf16[192,256]{1,0:T(8,128)(2,1)} %bitcast.10, f32[1,64]{1,0:T(1,128)} %bitcast.12, f32[1,64]{1,0:T(1,128)} %bitcast.13, bf16[1024,256]{1,0:T(8,128)(2,1)} %w_ref.1, f32[1,2048]{1,0:T(1,128)} %bitcast.11, ...), custom_call_target="tpu_custom_call" | custom-call | tf_op jit(solution)/shard_map/pallas_call | solution.py:472
  27.6 0.9 %copy.10 = bf16[1,192,2048]{2,1,0:T(8,128)(2,1)} copy(bf16[1,192,2048]{2,1,0:T(8,128)(2,1)S(1)} %bitcast.7) | data formatting | bytes 1572864
